TPU v7x, 32 devices: a whole 2x2x4 slice. The times are simulated.
32 devices in a mesh: ep: 8 (over z, x), tp: 4 (over y, core).
Axes of the slice: x: 2, y: 2, z: 4, core: 2. Of those that a mesh axis runs over, the one named last changes fastest.
Arguments:
- hidden_in: bfloat16 [256, 4096], P('ep'), may hold values from -6 to 6
- norm_gain: float32 [4096], replicated, may hold values from 0.1 to 1.9
- group_ids: int32 [256], P('ep'), may hold values from 0 to 1, as said below
- inner_ids: int32 [256, 4], P('ep'), may hold values from 0 to 7, as said below
- group_prob: float32 [256], P('ep'), may hold values from 0.25 to 1
- expert_prob: float32 [256, 4], P('ep'), may hold values from 0.1 to 1
- w_gate: bfloat16 [16, 4096, 1024], P('ep', None, 'tp'), may hold values from -0.09375 to 0.09375
- w_up: bfloat16 [16, 4096, 1024], P('ep', None, 'tp'), may hold values from -0.09375 to 0.09375
- w_down: bfloat16 [16, 1024, 4096], P('ep', None, 'tp'), may hold values from -0.1875 to 0.1875
Outputs:
- moe_out: bfloat16 [256, 4096], P('ep', 'tp')
Inputs may be any that keep to these rules, and one draw needn't show every extreme that they name: `group_ids`: among the 32 tokens of one index of ep no group is named by more than 16 tokens; one group is named by exactly 16 of them, and all of these name one common expert of it. `inner_ids`: each row names 4 different experts of the token's group.
All inputs are finite; a program needn't handle non-finite values.
Results may differ from a plain program's by a relative error of at most 0.0069.
Values may be sent and summed in bfloat16 or wider, within the bound.
A program may use at most 64 MiB of HBM per device.

v0:
```python
import functools

import jax
import jax.numpy as jnp
from jax import lax
from jax.experimental import pallas as pl
from jax.experimental.pallas import tpu as pltpu
from jax.sharding import PartitionSpec as P

EPG = 8
EPS = 1e-06
CORES = 2
LANES = 128
MESH = pl.DeviceIdType.MESH


def rem(value, count):
    return lax.rem(value + count, count)


def moe_kernel(
    ep_count, tp_count,
    hid_ref, gain_ref, grp_ref, inner_ref, gprob_ref, eprob_ref, wg_hbm, wu_hbm, wd_hbm,
    out_ref,
    wg, wu, wd, rows_out, rows_in, acts, parts, back,
    w_sem, a_send, a_recv, b_send, b_recv, r_send, r_recv,
    h_send, h_recv, hr_send, hr_recv, o_send, o_recv,
):
    experts, depth, hidden = wg.shape
    ranks = EPG // experts
    groups = ep_count // ranks
    ys = tp_count // CORES
    tokens = hid_ref.shape[0]
    cap = tokens // 2
    feats = depth // tp_count
    cols = wd.shape[2]

    me_ep, me_tp = lax.axis_index("ep"), lax.axis_index("tp")
    g, p = lax.div(me_ep, ranks), lax.rem(me_ep, ranks)
    y, c = lax.div(me_tp, CORES), lax.rem(me_tp, CORES)
    sib = 1 - c

    loads = []
    for k, (src, dst) in enumerate(((wg_hbm, wg), (wu_hbm, wu), (wd_hbm, wd))):
        load = pltpu.make_async_copy(src, dst, w_sem.at[k])
        load.start()
        loads.append(load)

    barrier = pltpu.get_barrier_semaphore()
    partners = 0

    def shift(rank, d, sign):
        return rem(lax.div(rank, 2) + sign * (d // 2), ranks // 2) * 2 + rem(
            lax.rem(rank, 2) + sign * (d % 2), 2
        )

    def to(d):
        return shift(p, d, 1)

    def of(d):
        return shift(p, d, -1)

    def mate(j, rank):
        flip = groups == 2 and ranks > 2 and j == 1
        return shift(rank, ranks // 2, 1) if flip else rank

    def greet(ep, tp):
        pl.semaphore_signal(
            barrier, inc=1, device_id={"ep": ep, "tp": tp}, device_id_type=MESH
        )

    for d in range(1, ep_count):
        greet(rem(me_ep + d, ep_count), me_tp)
        partners += 1
    for d in range(ranks):
        for dy in range(1, ys):
            greet(g * ranks + to(d), rem(y + dy, ys) * CORES + c)
            partners += 1
    greet(me_ep, y * CORES + sib)
    partners += 1

    x = hid_ref[...].astype(jnp.float32)
    scale = lax.rsqrt(jnp.mean(x * x, axis=-1, keepdims=True) + EPS)
    mine = pl.ds(pl.multiple_of(me_tp * feats, LANES), feats)
    normed = (
        hid_ref[:, mine].astype(jnp.float32) * scale * gain_ref[:, mine]
    ).astype(jnp.bfloat16)

    r0 = lax.broadcasted_iota(jnp.int32, (tokens, tokens), 0)
    r1 = lax.broadcasted_iota(jnp.int32, (tokens, tokens), 1)
    grow = jnp.broadcast_to(grp_ref[...], (tokens, tokens))
    gcol = jnp.sum(jnp.where(r0 == r1, grow, 0), axis=1, keepdims=True)
    same = gcol == grow
    rank_row = jnp.sum(jnp.where(same & (r0 < r1), 1, 0), axis=0, keepdims=True)
    rank_col = jnp.sum(jnp.where(same & (r1 < r0), 1, 0), axis=1, keepdims=True)

    def slot(group, rank):
        rel = g - group
        return jnp.where(rel < 0, rel + groups, rel) * cap + rank

    slots = groups * cap
    pick = (
        lax.broadcasted_iota(jnp.int32, (slots, tokens), 0) == slot(grp_ref[...], rank_row)
    ).astype(jnp.bfloat16)

    line = lax.broadcasted_iota(jnp.int32, (LANES, tokens), 0)
    inner, eprob, prob = inner_ref[...], eprob_ref[...], gprob_ref[...]
    weight = jnp.zeros((LANES, tokens), jnp.float32)
    for k in range(inner.shape[0]):
        hit = lax.rem(line, EPG) == inner[k : k + 1, :]
        weight += jnp.where(hit, prob * eprob[k : k + 1, :], 0.0)
    high = weight.astype(jnp.bfloat16).astype(jnp.float32)
    mid = (weight - high).astype(jnp.bfloat16).astype(jnp.float32)
    low = weight - high - mid
    part = lax.div(line, EPG)
    weight = jnp.where(
        part == 0, high, jnp.where(part == 1, mid, jnp.where(part == 2, low, 0.0))
    ).astype(jnp.bfloat16)

    data = jnp.dot(pick, normed, preferred_element_type=jnp.float32).astype(jnp.bfloat16)
    wdat = lax.dot_general(
        pick, weight, (((1,), (1,)), ((), ())), preferred_element_type=jnp.float32
    ).astype(jnp.bfloat16)
    my_rows = pl.ds(pl.multiple_of(p * cap, cap), cap)
    rows_in[0, c, y, my_rows, :feats] = data[:cap]
    rows_in[0, c, y, my_rows, feats:] = wdat[:cap]
    for j in range(1, groups):
        rows_out[j, :, :feats] = data[j * cap : (j + 1) * cap]
        rows_out[j, :, feats:] = wdat[j * cap : (j + 1) * cap]

    pl.semaphore_wait(barrier, partners)
    sent = []

    def send(src, dst, ssem, rsem, ep, tp):
        copy = pltpu.make_async_remote_copy(
            src_ref=src, dst_ref=dst, send_sem=ssem, recv_sem=rsem,
            device_id={"ep": ep, "tp": tp}, device_id_type=MESH,
        )
        copy.start()
        sent.append(copy)

    def landed(dst, ssem, rsem):
        pltpu.make_async_remote_copy(
            src_ref=dst, dst_ref=dst, send_sem=ssem, recv_sem=rsem,
            device_id={"ep": me_ep, "tp": me_tp}, device_id_type=MESH,
        ).wait_recv()

    def piece(j, core, yy, rank):
        return rows_in.at[j, core, yy, pl.ds(pl.multiple_of(rank * cap, cap), cap)]

    hops = sorted(
        ((d, dy) for d in range(ranks) for dy in range(ys)),
        key=lambda h: (h != (0, 0), -(h[0] // 2 + h[0] % 2 + h[1])),
    )

    def spread(j):
        own = piece(j, c, y, p)
        for d, dy in hops[1:]:
            send(own, own, b_send.at[j, d, dy], b_recv.at[j, d, dy],
                 g * ranks + to(d), rem(y + dy, ys) * CORES + c)
        send(own, own, r_send.at[j, 0, 0], r_recv.at[j, 0, 0], me_ep, y * CORES + sib)

    def relay(j):
        for d, dy in hops[1:]:
            got = piece(j, c, rem(y - dy, ys), of(d))
            landed(got, b_send.at[j, d, dy], b_recv.at[j, d, dy])
            send(got, got, r_send.at[j, d, dy], r_recv.at[j, d, dy], me_ep, y * CORES + sib)

    def expand(j):
        gates = [jnp.zeros((ranks * cap, hidden), jnp.float32) for _ in range(experts)]
        ups = [jnp.zeros((ranks * cap, hidden), jnp.float32) for _ in range(experts)]
        for half in range(CORES):
            core = sib if half else c
            if half:
                for d, dy in hops:
                    landed(piece(j, sib, rem(y - dy, ys), of(d)),
                           r_send.at[j, d, dy], r_recv.at[j, d, dy])
            for yy in range(ys):
                lhs = rows_in[j, core, yy, :, :feats]
                ks = pl.ds(pl.multiple_of((yy * CORES + core) * feats, feats), feats)
                for e in range(experts):
                    gates[e] += jnp.dot(lhs, wg[e, ks, :], preferred_element_type=jnp.float32)
                    ups[e] += jnp.dot(lhs, wu[e, ks, :], preferred_element_type=jnp.float32)
        wrow = rows_in[j, 0, 0, :, feats:].astype(jnp.float32)
        lanes = lax.broadcasted_iota(jnp.int32, wrow.shape, 1)
        for e in range(experts):
            w = jnp.sum(
                jnp.where(lax.rem(lanes, EPG) == p * experts + e, wrow, 0.0),
                axis=1, keepdims=True,
            )
            act = gates[e] / (1.0 + jnp.exp(-gates[e])) * ups[e] * w
            acts[j, c, y, :, e * hidden : (e + 1) * hidden] = act.astype(jnp.bfloat16)
        own = acts.at[j, c, y]
        for dy in range(1, ys):
            send(own, own, h_send.at[j, dy], h_recv.at[j, dy], me_ep,
                 rem(y + dy, ys) * CORES + c)
        send(own, own, hr_send.at[j, 0], hr_recv.at[j, 0], me_ep, y * CORES + sib)

    def act_relay(j):
        for dy in range(1, ys):
            got = acts.at[j, c, rem(y - dy, ys)]
            landed(got, h_send.at[j, dy], h_recv.at[j, dy])
            send(got, got, hr_send.at[j, dy], hr_recv.at[j, dy], me_ep, y * CORES + sib)

    def contract(j):
        total = jnp.zeros((ranks * cap, cols), jnp.float32)
        for half in range(CORES):
            core = sib if half else c
            if half:
                for dy in range(ys):
                    landed(acts.at[j, sib, rem(y - dy, ys)], hr_send.at[j, dy], hr_recv.at[j, dy])
            for yy in range(ys):
                ks = pl.ds(pl.multiple_of((yy * CORES + core) * hidden, hidden), hidden)
                for e in range(experts):
                    total += jnp.dot(
                        acts[j, core, yy, :, e * hidden : (e + 1) * hidden],
                        wd[e, ks, :], preferred_element_type=jnp.float32,
                    )
        parts[j] = total.astype(jnp.bfloat16)
        source = rem(g + j, groups) * ranks
        for d in reversed(range(ranks)):
            rows = pl.ds(pl.multiple_of(to(d) * cap, cap), cap)
            if j == 0 and d == 0:
                back[0, p] = parts[0, rows, :]
            else:
                send(parts.at[j, rows], back.at[j, p], o_send.at[j, d], o_recv.at[j, d],
                     source + mate(j, to(d)), me_tp)

    for j in range(1, groups):
        send(rows_out.at[j], piece(j, c, y, mate(j, p)), a_send.at[j],
             a_recv.at[j], rem(g - j, groups) * ranks + mate(j, p), me_tp)
    spread(0)
    for j in range(groups):
        if j + 1 < groups:
            landed(piece(j + 1, c, y, p), a_send.at[j + 1], a_recv.at[j + 1])
            spread(j + 1)
        relay(j)
        if j == 0:
            loads[0].wait()
            loads[1].wait()
        else:
            act_relay(j - 1)
        expand(j)
        if j == 0:
            loads[2].wait()
        else:
            contract(j - 1)
    act_relay(groups - 1)
    contract(groups - 1)

    sums = []
    for j in range(groups):
        for d in range(ranks):
            if j or d:
                landed(back.at[j, shift(mate(j, p), d, -1)], o_send.at[j, d], o_recv.at[j, d])
        block = back[j, 0].astype(jnp.float32)
        for k in range(1, ranks):
            block += back[j, k].astype(jnp.float32)
        sums.append(block.astype(jnp.bfloat16))
    place = (
        lax.broadcasted_iota(jnp.int32, (tokens, slots), 1) == slot(gcol, rank_col)
    ).astype(jnp.bfloat16)
    out_ref[...] = jnp.dot(
        place, jnp.concatenate(sums, axis=0), preferred_element_type=jnp.float32
    ).astype(jnp.bfloat16)
    for copy in sent:
        copy.wait_send()


def solution(mesh):
    ep_count, tp_count = mesh.shape["ep"], mesh.shape["tp"]

    def on_device(
        hidden_in, norm_gain, group_ids, inner_ids, group_prob, expert_prob, w_gate, w_up, w_down
    ):
        tokens = hidden_in.shape[0]
        experts, depth, hidden = w_gate.shape
        cols = w_down.shape[2]
        ranks, cap = EPG // experts, tokens // 2
        groups, ys = ep_count // ranks, tp_count // CORES
        feats = depth // tp_count
        vmem = pl.BlockSpec(memory_space=pltpu.VMEM)
        hbm = pl.BlockSpec(memory_space=pl.ANY)
        dma = pltpu.SemaphoreType.DMA
        return pl.pallas_call(
            functools.partial(moe_kernel, ep_count, tp_count),
            out_shape=jax.ShapeDtypeStruct((tokens, cols), jnp.bfloat16),
            in_specs=[vmem] * 6 + [hbm] * 3,
            out_specs=vmem,
            scratch_shapes=[
                pltpu.VMEM(w_gate.shape, jnp.bfloat16),
                pltpu.VMEM(w_up.shape, jnp.bfloat16),
                pltpu.VMEM(w_down.shape, jnp.bfloat16),
                pltpu.VMEM((groups, cap, feats + LANES), jnp.bfloat16),
                pltpu.VMEM((groups, CORES, ys, ranks * cap, feats + LANES), jnp.bfloat16),
                pltpu.VMEM((groups, CORES, ys, ranks * cap, experts * hidden), jnp.bfloat16),
                pltpu.VMEM((groups, ranks * cap, cols), jnp.bfloat16),
                pltpu.VMEM((groups, ranks, cap, cols), jnp.bfloat16),
                dma((3,)),
                dma((groups,)), dma((groups,)),
                dma((groups, ranks, ys)), dma((groups, ranks, ys)),
                dma((groups, ranks, ys)), dma((groups, ranks, ys)),
                dma((groups, ys)), dma((groups, ys)),
                dma((groups, ys)), dma((groups, ys)),
                dma((groups, ranks)), dma((groups, ranks)),
            ],
            compiler_params=pltpu.CompilerParams(
                collective_id=0, has_side_effects=True, vmem_limit_bytes=56 * 1024 * 1024
            ),
        )(
            hidden_in, norm_gain.reshape(1, depth), group_ids.reshape(1, tokens), inner_ids.T,
            group_prob.reshape(1, tokens), expert_prob.T, w_gate, w_up, w_down,
        )

    placed = (
        P("ep", None), P(), P("ep"), P("ep", None), P("ep"), P("ep", None),
        P("ep", None, "tp"), P("ep", None, "tp"), P("ep", None, "tp"),
    )
    return jax.shard_map(
        on_device, mesh=mesh, in_specs=placed, out_specs=P("ep", "tp"), check_vma=False
    )
```

profile of v0, /device:TPU:0, one launch (start us, length us, event | category | flops | bytes accessed | tf_op | source)
XLA Modules:
  0.0 33.9 jit_solution(10986459717290416508)
XLA Ops:
  0.0 32.4 %shard_map.91 = bf16[32,1024]{1,0:T(8,128)(2,1)} custom-call(bf16[32,4096]{1,0:T(8,128)(2,1)} %hid_ref.1, f32[1,4096]{1,0:T(1,128)} %bitcast.5, s32[1,32]{1,0:T(1,128)} %bitcast.8, s32[4,32]{1,0:T(4,128)} %bitcast.6, f32[1,32]{1,0:T(1,128)} %bitcast.9, f32[4,32]{1,0:T(4,128)} %bitcast.7, bf16[2,4096,256]{2,1,0:T(8,128)(2,1)} %wg_hbm.1, ...), custom_call_target="tpu_custom_call" | custom-call | tf_op jit(solution)/shard_map/pallas_call | solution.py:285
  32.4 1.5 %copy.11 = bf16[32,1024]{1,0:T(8,128)(2,1)} copy(bf16[32,1024]{1,0:T(8,128)(2,1)} %shard_map.91) | data formatting | bytes 131072
where the time goes:
time: 34.1 us; the launch traced here: 33.9 us
  Pallas kernels  32.4 us (95%)
  local copies, waits for them, and re-layouts  1.47 us (4%)
    pallas_call x1, Pallas kernels, on_device(): pl.pallas_call(functools.partial(moe_kernel, ep_count, tp_count), out_sha...  32.4 us
    unnamed x1, local copies, waits for them, and re-layouts  1.47 us

commit v1 on v0

--- a/solution.py
+++ b/solution.py
@@ -238,14 +238,15 @@
         if j == 0:
             loads[0].wait()
             loads[1].wait()
-        else:
+        expand(j)
+        if j:
             act_relay(j - 1)
-        expand(j)
-        if j == 0:
-            loads[2].wait()
-        else:
+            if j == 1:
+                loads[2].wait()
             contract(j - 1)
     act_relay(groups - 1)
+    if groups == 1:
+        loads[2].wait()
     contract(groups - 1)
 
     sums = []
@@ -284,7 +285,7 @@
         dma = pltpu.SemaphoreType.DMA
         return pl.pallas_call(
             functools.partial(moe_kernel, ep_count, tp_count),
-            out_shape=jax.ShapeDtypeStruct((tokens, cols), jnp.bfloat16),
+            out_shape=pltpu.VMEM((tokens, cols), jnp.bfloat16),
             in_specs=[vmem] * 6 + [hbm] * 3,
             out_specs=vmem,
             scratch_shapes=[

time: 34.1 us -> 31.5 us (0.924)
  Pallas kernels: 32.4 us -> 30.7 us
  local copies, waits for them, and re-layouts: 1.47 us -> 0.63 us
    pallas_call x1, Pallas kernels: 32.4 us -> 30.7 us  [on_device(): pl.pallas_call(functools.partial(moe_kernel, ep_count, tp_count), out_sha...]
    unnamed x1, local copies, waits for them, and re-layouts: 1.47 us -> 0.63 us
where the time goes in v1:
time: 31.5 us; the launch traced here: 31.3 us
  Pallas kernels  30.7 us (97%)
  local copies, waits for them, and re-layouts  0.63 us (2%)
    pallas_call x1, Pallas kernels, on_device(): pl.pallas_call(functools.partial(moe_kernel, ep_count, tp_count), out_sha...  30.7 us
    unnamed x1, local copies, waits for them, and re-layouts  0.63 us

profile of v1, /device:TPU:0, one launch (start us, length us, event | category | flops | bytes accessed | tf_op | source)
XLA Modules:
  0.0 31.3 jit_solution(6897794979955729614)
XLA Ops:
  0.0 30.7 %shard_map.91 = bf16[32,1024]{1,0:T(8,128)(2,1)S(1)} custom-call(bf16[32,4096]{1,0:T(8,128)(2,1)} %hid_ref.1, f32[1,4096]{1,0:T(1,128)} %bitcast.5, s32[1,32]{1,0:T(1,128)} %bitcast.8, s32[4,32]{1,0:T(4,128)} %bitcast.6, f32[1,32]{1,0:T(1,128)} %bitcast.9, f32[4,32]{1,0:T(4,128)} %bitcast.7, bf16[2,4096,256]{2,1,0:T(8,128)(2,1)} %wg_hbm.1, ...), custom_call_target="tpu_custom_call" | custom-call | tf_op jit(solution)/shard_map/pallas_call | solution.py:286
  30.7 0.6 %copy.11 = bf16[32,1024]{1,0:T(8,128)(2,1)} copy(bf16[32,1024]{1,0:T(8,128)(2,1)S(1)} %shard_map.91) | data formatting | bytes 131072

commit v2 on v1

v2 whole, which is shorter than its diff:
```python
import functools

import jax
import jax.numpy as jnp
from jax import lax
from jax.experimental import pallas as pl
from jax.experimental.pallas import tpu as pltpu
from jax.sharding import PartitionSpec as P

EPG = 8
EPS = 1e-06
CORES = 2
LANES = 128
SPLIT = 1
MESH = pl.DeviceIdType.MESH


def rem(value, count):
    return lax.rem(value + count, count)


def moe_kernel(
    ep_count, tp_count,
    hid_hbm, gain_hbm, grp_hbm, inner_hbm, gprob_hbm, eprob_hbm, wg_hbm, wu_hbm, wd_hbm,
    out_ref,
    hid_ref, gain_ref, grp_ref, inner_ref, gprob_ref, eprob_ref,
    wg, wu, wd, rows_out, rows_own, rows_in, acts, parts, back,
    i_sem, w_sem, a_send, a_recv, s_send, s_recv, q_send, q_recv, b_send, b_recv, r_send, r_recv,
    h_send, h_recv, hr_send, hr_recv, o_send, o_recv,
):
    experts, depth, hidden = wg.shape
    ranks = EPG // experts
    groups = ep_count // ranks
    ys = tp_count // CORES
    tokens = hid_ref.shape[0]
    cap = tokens // 2
    feats = depth // tp_count
    side = depth // CORES
    cols = wd.shape[2]
    block = cols // SPLIT

    me_ep, me_tp = lax.axis_index("ep"), lax.axis_index("tp")
    g, p = lax.div(me_ep, ranks), lax.rem(me_ep, ranks)
    y, c = lax.div(me_tp, CORES), lax.rem(me_tp, CORES)
    sib = 1 - c

    barrier = pltpu.get_barrier_semaphore()
    partners = 0

    def shift(rank, d, sign):
        return rem(lax.div(rank, 2) + sign * (d // 2), ranks // 2) * 2 + rem(
            lax.rem(rank, 2) + sign * (d % 2), 2
        )

    def to(d):
        return shift(p, d, 1)

    def of(d):
        return shift(p, d, -1)

    def mate(j, rank):
        flip = groups == 2 and ranks > 2 and j == 1
        return shift(rank, ranks // 2, 1) if flip else rank

    def twin(dy=0):
        return rem(y + dy, ys) * CORES + sib

    def greet(ep, tp):
        pl.semaphore_signal(
            barrier, inc=1, device_id={"ep": ep, "tp": tp}, device_id_type=MESH
        )

    for d in range(1, ep_count):
        greet(rem(me_ep + d, ep_count), me_tp)
        partners += 1
    for j in range(1, groups):
        greet(rem(g - j, groups) * ranks + mate(j, p), twin())
        partners += 1
    for d in range(ranks):
        for dy in range(ys):
            greet(g * ranks + to(d), twin(dy))
            partners += 1

    fetched = []
    for k, (src, dst) in enumerate((
        (hid_hbm, hid_ref), (gain_hbm, gain_ref), (grp_hbm, grp_ref), (inner_hbm, inner_ref),
        (gprob_hbm, gprob_ref), (eprob_hbm, eprob_ref),
    )):
        load = pltpu.make_async_copy(src, dst, i_sem.at[k])
        load.start()
        fetched.append(load)
    for load in fetched:
        load.wait()
    loads = []
    for k, (src, dst) in enumerate(((wg_hbm, wg), (wu_hbm, wu), (wd_hbm, wd))):
        load = pltpu.make_async_copy(src, dst, w_sem.at[k])
        load.start()
        loads.append(load)

    r0 = lax.broadcasted_iota(jnp.int32, (tokens, tokens), 0)
    r1 = lax.broadcasted_iota(jnp.int32, (tokens, tokens), 1)
    grow = jnp.broadcast_to(grp_ref[...], (tokens, tokens))
    gcol = jnp.sum(jnp.where(r0 == r1, grow, 0), axis=1, keepdims=True)
    same = gcol == grow
    rank_row = jnp.sum(jnp.where(same & (r0 < r1), 1, 0), axis=0, keepdims=True)
    rank_col = jnp.sum(jnp.where(same & (r1 < r0), 1, 0), axis=1, keepdims=True)

    def slot(group, rank):
        rel = g - group
        return jnp.where(rel < 0, rel + groups, rel) * cap + rank

    slots = groups * cap
    pick = (
        lax.broadcasted_iota(jnp.int32, (slots, tokens), 0) == slot(grp_ref[...], rank_row)
    ).astype(jnp.bfloat16)

    line = lax.broadcasted_iota(jnp.int32, (LANES, tokens), 0)
    inner, eprob, prob = inner_ref[...], eprob_ref[...], gprob_ref[...]
    weight = jnp.zeros((LANES, tokens), jnp.float32)
    for k in range(inner.shape[0]):
        hit = lax.rem(line, EPG) == inner[k : k + 1, :]
        weight += jnp.where(hit, prob * eprob[k : k + 1, :], 0.0)
    high = weight.astype(jnp.bfloat16).astype(jnp.float32)
    mid = (weight - high).astype(jnp.bfloat16).astype(jnp.float32)
    low = weight - high - mid
    part = lax.div(line, EPG)
    weight = jnp.where(
        part == 0, high, jnp.where(part == 1, mid, jnp.where(part == 2, low, 0.0))
    ).astype(jnp.bfloat16)
    wdat = lax.dot_general(
        pick, weight, (((1,), (1,)), ((), ())), preferred_element_type=jnp.float32
    ).astype(jnp.bfloat16)

    x = hid_ref[...].astype(jnp.float32)
    scale = lax.rsqrt(jnp.mean(x * x, axis=-1, keepdims=True) + EPS)

    def normed(cut):
        return (
            hid_ref[:, cut].astype(jnp.float32) * scale * gain_ref[:, cut]
        ).astype(jnp.bfloat16)

    if groups > 1:
        mine = pl.ds(pl.multiple_of(me_tp * feats, LANES), feats)
        data = jnp.dot(
            pick[cap:], normed(mine), preferred_element_type=jnp.float32
        ).astype(jnp.bfloat16)
        for j in range(1, groups):
            rows_out[j, :, :feats] = data[(j - 1) * cap : j * cap]
            rows_out[j, :, feats:] = wdat[j * cap : (j + 1) * cap]

    with jax.named_scope("barrier"):
        pl.semaphore_wait(barrier, partners)
    sent = []

    def send(src, dst, ssem, rsem, ep, tp):
        copy = pltpu.make_async_remote_copy(
            src_ref=src, dst_ref=dst, send_sem=ssem, recv_sem=rsem,
            device_id={"ep": ep, "tp": tp}, device_id_type=MESH,
        )
        copy.start()
        sent.append(copy)

    def landed(dst, ssem, rsem):
        pltpu.make_async_remote_copy(
            src_ref=dst, dst_ref=dst, send_sem=ssem, recv_sem=rsem,
            device_id={"ep": me_ep, "tp": me_tp}, device_id_type=MESH,
        ).wait_recv()

    def lines(rank):
        return pl.ds(pl.multiple_of(rank * cap, cap), cap)

    def piece(j, core, yy, rank):
        return rows_in.at[j, core, yy, lines(rank)]

    def own(core, rank):
        return rows_own.at[core, lines(rank)]

    for j in range(1, groups):
        send(rows_out.at[j], piece(j, c, y, mate(j, p)), a_send.at[j],
             a_recv.at[j], rem(g - j, groups) * ranks + mate(j, p), twin())

    for core in range(CORES):
        cut = slice(core * side, (core + 1) * side)
        rows_own[core, lines(p), :side] = jnp.dot(
            pick[:cap], normed(cut), preferred_element_type=jnp.float32
        ).astype(jnp.bfloat16)
        rows_own[core, lines(p), side:] = wdat[:cap]

    near = sorted(range(1, ranks), key=lambda d: -(d // 2 + d % 2))
    hops = sorted(
        ((d, dy) for d in range(ranks) for dy in range(ys)),
        key=lambda h: (h != (0, 0), -(h[0] // 2 + h[0] % 2 + h[1])),
    )

    for d in near:
        send(own(c, p), own(c, p), s_send.at[d], s_recv.at[d], g * ranks + to(d), twin())

    def relay_own():
        for d in near:
            got = own(sib, of(d))
            landed(got, s_send.at[d], s_recv.at[d])
            send(got, got, q_send.at[d], q_recv.at[d], me_ep, twin())

    def spread(j):
        held = piece(j, sib, y, p)
        for d, dy in hops[1:]:
            send(held, held, b_send.at[j, d, dy], b_recv.at[j, d, dy], g * ranks + to(d), twin(dy))
        send(held, held, r_send.at[j, 0, 0], r_recv.at[j, 0, 0], me_ep, twin())

    def relay(j):
        for d, dy in hops[1:]:
            got = piece(j, c, rem(y - dy, ys), of(d))
            landed(got, b_send.at[j, d, dy], b_recv.at[j, d, dy])
            send(got, got, r_send.at[j, d, dy], r_recv.at[j, d, dy], me_ep, twin())

    def expand(j):
        gates = [jnp.zeros((ranks * cap, hidden), jnp.float32) for _ in range(experts)]
        ups = [jnp.zeros((ranks * cap, hidden), jnp.float32) for _ in range(experts)]

        def multiply(lhs, ks):
            for e in range(experts):
                gates[e] += jnp.dot(lhs, wg[e, ks, :], preferred_element_type=jnp.float32)
                ups[e] += jnp.dot(lhs, wu[e, ks, :], preferred_element_type=jnp.float32)

        if j == 0:
            for core in (sib, c):
                if core is c:
                    for d in near:
                        landed(own(c, of(d)), q_send.at[d], q_recv.at[d])
                multiply(rows_own[core, :, :side], pl.ds(pl.multiple_of(core * side, side), side))
            wrow = rows_own[sib, :, side:].astype(jnp.float32)
        else:
            landed(piece(j, c, y, p), r_send.at[j, 0, 0], r_recv.at[j, 0, 0])
            for core in (c, sib):
                if core is sib:
                    for d, dy in hops[1:]:
                        landed(piece(j, sib, rem(y - dy, ys), of(d)),
                               r_send.at[j, d, dy], r_recv.at[j, d, dy])
                for yy in range(ys):
                    ks = pl.ds(pl.multiple_of((yy * CORES + core) * feats, feats), feats)
                    multiply(rows_in[j, core, yy, :, :feats], ks)
            wrow = rows_in[j, c, 0, :, feats:].astype(jnp.float32)
        lanes = lax.broadcasted_iota(jnp.int32, wrow.shape, 1)
        for e in range(experts):
            w = jnp.sum(
                jnp.where(lax.rem(lanes, EPG) == p * experts + e, wrow, 0.0),
                axis=1, keepdims=True,
            )
            act = gates[e] / (1.0 + jnp.exp(-gates[e])) * ups[e] * w
            acts[j, c, y, :, e * hidden : (e + 1) * hidden] = act.astype(jnp.bfloat16)
        held = acts.at[j, c, y]
        for dy in range(1, ys):
            send(held, held, h_send.at[j, dy], h_recv.at[j, dy], me_ep, twin(dy))
        send(held, held, hr_send.at[j, 0], hr_recv.at[j, 0], me_ep, twin())

    def act_relay(j):
        for dy in range(1, ys):
            got = acts.at[j, sib, rem(y - dy, ys)]
            landed(got, h_send.at[j, dy], h_recv.at[j, dy])
            send(got, got, hr_send.at[j, dy], hr_recv.at[j, dy], me_ep, twin())

    def contract(j):
        total = jnp.zeros((ranks * cap, cols), jnp.float32)

        def multiply(core, yy, cut, total):
            ks = pl.ds(pl.multiple_of((yy * CORES + core) * hidden, hidden), hidden)
            for e in range(experts):
                total += jnp.dot(
                    acts[j, core, yy, :, e * hidden : (e + 1) * hidden],
                    wd[e, ks, cut], preferred_element_type=jnp.float32,
                )
            return total

        whole = slice(0, cols)
        total = multiply(c, y, whole, total)
        for dy in range(1, ys):
            total = multiply(sib, rem(y - dy, ys), whole, total)
        landed(acts.at[j, sib, y], hr_send.at[j, 0], hr_recv.at[j, 0])
        total = multiply(sib, y, whole, total)
        for dy in range(1, ys):
            landed(acts.at[j, c, rem(y - dy, ys)], hr_send.at[j, dy], hr_recv.at[j, dy])
        source = rem(g + j, groups) * ranks
        for b in range(SPLIT):
            cut = slice(b * block, (b + 1) * block)
            piece_total = total[:, cut]
            for dy in range(1, ys):
                piece_total = multiply(c, rem(y - dy, ys), cut, piece_total)
            parts[j, :, cut] = piece_total.astype(jnp.bfloat16)
            for d in reversed(range(ranks)):
                rows = lines(to(d))
                if j == 0 and d == 0:
                    back[0, p, :, cut] = parts[0, rows, cut]
                else:
                    send(parts.at[j, rows, cut], back.at[j, p, :, cut],
                         o_send.at[j, d, b], o_recv.at[j, d, b],
                         source + mate(j, to(d)), me_tp)

    for j in range(groups):
        if j + 1 < groups:
            with jax.named_scope(f"a_wait{j+1}"):
                landed(piece(j + 1, sib, y, p), a_send.at[j + 1], a_recv.at[j + 1])
            spread(j + 1)
        with jax.named_scope(f"relay{j}"):
            if j == 0:
                relay_own()
                loads[0].wait()
                loads[1].wait()
            else:
                relay(j)
        with jax.named_scope(f"expand{j}"):
            expand(j)
        if j:
            with jax.named_scope(f"act_relay{j-1}"):
                act_relay(j - 1)
            if j == 1:
                loads[2].wait()
            with jax.named_scope(f"contract{j-1}"):
                contract(j - 1)
    with jax.named_scope("act_relayL"):
        act_relay(groups - 1)
    if groups == 1:
        loads[2].wait()
    with jax.named_scope("contractL"):
        contract(groups - 1)

    sums = []
    for j in range(groups):
        with jax.named_scope(f"back{j}"):
            for b in range(SPLIT):
                for d in range(ranks):
                    if j or d:
                        landed(
                            back.at[j, shift(mate(j, p), d, -1), :, b * block : (b + 1) * block],
                            o_send.at[j, d, b], o_recv.at[j, d, b],
                        )
        total = back[j, 0].astype(jnp.float32)
        for k in range(1, ranks):
            total += back[j, k].astype(jnp.float32)
        sums.append(total.astype(jnp.bfloat16))
    with jax.named_scope("final"):
        place = (
            lax.broadcasted_iota(jnp.int32, (tokens, slots), 1) == slot(gcol, rank_col)
        ).astype(jnp.bfloat16)
        out_ref[...] = jnp.dot(
            place, jnp.concatenate(sums, axis=0), preferred_element_type=jnp.float32
        ).astype(jnp.bfloat16)
        for copy in sent:
            copy.wait_send()


def solution(mesh):
    ep_count, tp_count = mesh.shape["ep"], mesh.shape["tp"]

    def on_device(
        hidden_in, norm_gain, group_ids, inner_ids, group_prob, expert_prob, w_gate, w_up, w_down
    ):
        tokens = hidden_in.shape[0]
        experts, depth, hidden = w_gate.shape
        cols = w_down.shape[2]
        ranks, cap = EPG // experts, tokens // 2
        groups, ys = ep_count // ranks, tp_count // CORES
        feats, side = depth // tp_count, depth // CORES
        hbm = pl.BlockSpec(memory_space=pl.ANY)
        dma = pltpu.SemaphoreType.DMA
        small = (
            hidden_in, norm_gain.reshape(1, depth), group_ids.reshape(1, tokens), inner_ids.T,
            group_prob.reshape(1, tokens), expert_prob.T,
        )
        return pl.pallas_call(
            functools.partial(moe_kernel, ep_count, tp_count),
            out_shape=pltpu.VMEM((tokens, cols), jnp.bfloat16),
            in_specs=[hbm] * 9,
            out_specs=pl.BlockSpec(memory_space=pltpu.VMEM),
            scratch_shapes=[pltpu.VMEM(a.shape, a.dtype) for a in small] + [
                pltpu.VMEM(w_gate.shape, jnp.bfloat16),
                pltpu.VMEM(w_up.shape, jnp.bfloat16),
                pltpu.VMEM(w_down.shape, jnp.bfloat16),
                pltpu.VMEM((groups, cap, feats + LANES), jnp.bfloat16),
                pltpu.VMEM((CORES, ranks * cap, side + LANES), jnp.bfloat16),
                pltpu.VMEM((groups, CORES, ys, ranks * cap, feats + LANES), jnp.bfloat16),
                pltpu.VMEM((groups, CORES, ys, ranks * cap, experts * hidden), jnp.bfloat16),
                pltpu.VMEM((groups, ranks * cap, cols), jnp.bfloat16),
                pltpu.VMEM((groups, ranks, cap, cols), jnp.bfloat16),
                dma((len(small),)), dma((3,)),
                dma((groups,)), dma((groups,)),
                dma((ranks,)), dma((ranks,)),
                dma((ranks,)), dma((ranks,)),
                dma((groups, ranks, ys)), dma((groups, ranks, ys)),
                dma((groups, ranks, ys)), dma((groups, ranks, ys)),
                dma((groups, ys)), dma((groups, ys)),
                dma((groups, ys)), dma((groups, ys)),
                dma((groups, ranks, SPLIT)), dma((groups, ranks, SPLIT)),
            ],
            compiler_params=pltpu.CompilerParams(
                collective_id=0, has_side_effects=True, vmem_limit_bytes=56 * 1024 * 1024
            ),
        )(*small, w_gate, w_up, w_down)

    placed = (
        P("ep", None), P(), P("ep"), P("ep", None), P("ep"), P("ep", None),
        P("ep", None, "tp"), P("ep", None, "tp"), P("ep", None, "tp"),
    )
    return jax.shard_map(
        on_device, mesh=mesh, in_specs=placed, out_specs=P("ep", "tp"), check_vma=False
    )
```

time: 31.5 us -> 30.6 us (0.971)
  Pallas kernels: 30.7 us -> 29.8 us
    pallas_call x1, Pallas kernels: 30.7 us -> 29.8 us  [on_device(): pl.pallas_call(functools.partial(moe_kernel, ep_count, tp_count), out_sha...]
where the time goes in v2:
time: 30.6 us; the launch traced here: 30.5 us
  Pallas kernels  29.8 us (97%)
  local copies, waits for them, and re-layouts  0.63 us (2%)
    pallas_call x1, Pallas kernels, on_device(): pl.pallas_call(functools.partial(moe_kernel, ep_count, tp_count), out_sha...  29.8 us
    unnamed x1, local copies, waits for them, and re-layouts  0.63 us

profile of v2, /device:TPU:0, one launch (start us, length us, event | category | flops | bytes accessed | tf_op | source)
XLA Modules:
  0.0 30.5 jit_solution(6776590370632727805)
XLA Ops:
  0.0 29.8 %shard_map.91 = bf16[32,1024]{1,0:T(8,128)(2,1)S(1)} custom-call(bf16[32,4096]{1,0:T(8,128)(2,1)} %hid_hbm.1, f32[1,4096]{1,0:T(1,128)} %bitcast.5, s32[1,32]{1,0:T(1,128)} %bitcast.8, s32[4,32]{1,0:T(4,128)} %bitcast.6, f32[1,32]{1,0:T(1,128)} %bitcast.9, f32[4,32]{1,0:T(4,128)} %bitcast.7, bf16[2,4096,256]{2,1,0:T(8,128)(2,1)} %wg_hbm.1, ...), custom_call_target="tpu_custom_call" | custom-call | tf_op jit(solution)/shard_map/pallas_call | solution.py:369
  29.9 0.6 %copy.11 = bf16[32,1024]{1,0:T(8,128)(2,1)} copy(bf16[32,1024]{1,0:T(8,128)(2,1)S(1)} %shard_map.91) | data formatting | bytes 131072

commit v3 on v2

--- a/solution.py
+++ b/solution.py
@@ -11,7 +11,6 @@
 EPS = 1e-06
 CORES = 2
 LANES = 128
-SPLIT = 1
 MESH = pl.DeviceIdType.MESH
 
 
@@ -37,7 +36,6 @@
     feats = depth // tp_count
     side = depth // CORES
     cols = wd.shape[2]
-    block = cols // SPLIT
 
     me_ep, me_tp = lax.axis_index("ep"), lax.axis_index("tp")
     g, p = lax.div(me_ep, ranks), lax.rem(me_ep, ranks)
@@ -59,8 +57,7 @@
         return shift(p, d, -1)
 
     def mate(j, rank):
-        flip = groups == 2 and ranks > 2 and j == 1
-        return shift(rank, ranks // 2, 1) if flip else rank
+        return rank
 
     def twin(dy=0):
         return rem(y + dy, ys) * CORES + sib
@@ -70,9 +67,6 @@
             barrier, inc=1, device_id={"ep": ep, "tp": tp}, device_id_type=MESH
         )
 
-    for d in range(1, ep_count):
-        greet(rem(me_ep + d, ep_count), me_tp)
-        partners += 1
     for j in range(1, groups):
         greet(rem(g - j, groups) * ranks + mate(j, p), twin())
         partners += 1
@@ -279,21 +273,18 @@
         total = multiply(sib, y, whole, total)
         for dy in range(1, ys):
             landed(acts.at[j, c, rem(y - dy, ys)], hr_send.at[j, dy], hr_recv.at[j, dy])
-        source = rem(g + j, groups) * ranks
-        for b in range(SPLIT):
-            cut = slice(b * block, (b + 1) * block)
-            piece_total = total[:, cut]
-            for dy in range(1, ys):
-                piece_total = multiply(c, rem(y - dy, ys), cut, piece_total)
-            parts[j, :, cut] = piece_total.astype(jnp.bfloat16)
-            for d in reversed(range(ranks)):
-                rows = lines(to(d))
-                if j == 0 and d == 0:
-                    back[0, p, :, cut] = parts[0, rows, cut]
-                else:
-                    send(parts.at[j, rows, cut], back.at[j, p, :, cut],
-                         o_send.at[j, d, b], o_recv.at[j, d, b],
-                         source + mate(j, to(d)), me_tp)
+        for dy in range(1, ys):
+            total = multiply(c, rem(y - dy, ys), whole, total)
+        parts[j] = total.astype(jnp.bfloat16)
+        if j == 0:
+            for d in reversed(range(1, ranks)):
+                send(parts.at[0, lines(to(d))], back.at[0, p], o_send.at[0, d], o_recv.at[0, p],
+                     g * ranks + to(d), me_tp)
+            back[0, p] = parts[0, lines(p), :]
+            return
+        for r in range(ranks):
+            send(parts.at[j, lines(mate(j, r))], back.at[j, p], o_send.at[j, r], o_recv.at[j, p],
+                 rem(g + j, groups) * ranks + r, me_tp)
 
     for j in range(groups):
         if j + 1 < groups:
@@ -326,13 +317,9 @@
     sums = []
     for j in range(groups):
         with jax.named_scope(f"back{j}"):
-            for b in range(SPLIT):
-                for d in range(ranks):
-                    if j or d:
-                        landed(
-                            back.at[j, shift(mate(j, p), d, -1), :, b * block : (b + 1) * block],
-                            o_send.at[j, d, b], o_recv.at[j, d, b],
-                        )
+            for d in range(j == 0, ranks):
+                k = of(d) if j == 0 else d
+                landed(back.at[j, k], o_send.at[j, d], o_recv.at[j, k])
         total = back[j, 0].astype(jnp.float32)
         for k in range(1, ranks):
             total += back[j, k].astype(jnp.float32)
@@ -389,7 +376,7 @@
                 dma((groups, ranks, ys)), dma((groups, ranks, ys)),
                 dma((groups, ys)), dma((groups, ys)),
                 dma((groups, ys)), dma((groups, ys)),
-                dma((groups, ranks, SPLIT)), dma((groups, ranks, SPLIT)),
+                dma((groups, ranks)), dma((groups, ranks)),
             ],
             compiler_params=pltpu.CompilerParams(
                 collective_id=0, has_side_effects=True, vmem_limit_bytes=56 * 1024 * 1024

time: 30.6 us -> 29.5 us (0.964)
  Pallas kernels: 29.8 us -> 28.7 us
    pallas_call x1, Pallas kernels: 29.8 us -> 28.7 us  [on_device(): pl.pallas_call(functools.partial(moe_kernel, ep_count, tp_count), out_sha...]
where the time goes in v3:
time: 29.5 us; the launch traced here: 29.4 us
  Pallas kernels  28.7 us (97%)
  local copies, waits for them, and re-layouts  0.63 us (2%)
    pallas_call x1, Pallas kernels, on_device(): pl.pallas_call(functools.partial(moe_kernel, ep_count, tp_count), out_sha...  28.7 us
    unnamed x1, local copies, waits for them, and re-layouts  0.63 us

profile of v3, /device:TPU:0, one launch (start us, length us, event | category | flops | bytes accessed | tf_op | source)
XLA Modules:
  0.0 29.4 jit_solution(3593527681882711775)
XLA Ops:
  0.0 28.7 %shard_map.91 = bf16[32,1024]{1,0:T(8,128)(2,1)S(1)} custom-call(bf16[32,4096]{1,0:T(8,128)(2,1)} %hid_hbm.1, f32[1,4096]{1,0:T(1,128)} %bitcast.5, s32[1,32]{1,0:T(1,128)} %bitcast.8, s32[4,32]{1,0:T(4,128)} %bitcast.6, f32[1,32]{1,0:T(1,128)} %bitcast.9, f32[4,32]{1,0:T(4,128)} %bitcast.7, bf16[2,4096,256]{2,1,0:T(8,128)(2,1)} %wg_hbm.1, ...), custom_call_target="tpu_custom_call" | custom-call | tf_op jit(solution)/shard_map/pallas_call | solution.py:356
  28.7 0.6 %copy.11 = bf16[32,1024]{1,0:T(8,128)(2,1)} copy(bf16[32,1024]{1,0:T(8,128)(2,1)S(1)} %shard_map.91) | data formatting | bytes 131072
